TPU v7x, 32 devices: a whole 2x2x4 slice. The times are simulated.
32 devices in a mesh: grp: 2 (over x), tp: 16 (over z, y, core).
Axes of the slice: x: 2, y: 2, z: 4, core: 2. Of those that a mesh axis runs over, the one named last changes fastest.
Arguments:
- tokens: bfloat16 [160, 2048], P('grp', 'tp'), parts along dimension 0, may hold values from -6 to 6
- lengths: int32 [160], P('grp'), parts along dimension 0, may hold values from 1 to 4096, 81920 in all
- cell_memory: float32 [2, 160, 2048, 256], P(None, 'grp', 'tp'), parts along dimension 1, may hold values from -0.6 to 0.6
- key_sums: float32 [2, 160, 2048], P(None, 'grp', 'tp'), parts along dimension 1, may hold values from -3 to 3
- stabilizer: float32 [2, 160, 8], P(None, 'grp'), parts along dimension 1, may hold values from -3 to 1
- norm_gain: bfloat16 [2, 2048], replicated, may hold values from 0.099609375 to 1.8984375
- query_weight: bfloat16 [2, 2048, 2048], P(None, None, 'tp'), may hold values from -0.125 to 0.125
- key_weight: bfloat16 [2, 2048, 2048], P(None, None, 'tp'), may hold values from -0.125 to 0.125
- value_weight: bfloat16 [2, 2048, 2048], P(None, None, 'tp'), may hold values from -0.125 to 0.125
- outgate_weight: bfloat16 [2, 2048, 2048], P(None, None, 'tp'), may hold values from -0.125 to 0.125
- ingate_weight: bfloat16 [2, 2048, 8], replicated, may hold values from -0.125 to 0.125
- forget_weight: bfloat16 [2, 2048, 8], replicated, may hold values from -0.125 to 0.125
- ingate_bias: float32 [2, 8], replicated, may hold values from -3 to 3
- forget_bias: float32 [2, 8], replicated, may hold values from -1 to 4
- forget_slope: float32 [2, 8], replicated, may hold values from -3 to 3
- head_gain: bfloat16 [2, 2048], P(None, 'tp'), may hold values from 0.099609375 to 1.8984375
- output_weight: bfloat16 [2, 2048, 2048], P(None, None, 'tp'), may hold values from -0.125 to 0.125
Outputs:
- new_tokens: bfloat16 [160, 2048], P('grp', 'tp'), parts along dimension 0
- new_memory: float32 [2, 160, 2048, 256], P(None, 'grp', 'tp'), parts along dimension 1
- new_key_sums: float32 [2, 160, 2048], P(None, 'grp', 'tp'), parts along dimension 1
- new_stabilizer: float32 [2, 160, 8], P(None, 'grp'), parts along dimension 1
There are 2 independent parts, one for each index of `grp`. A program takes and returns all parts, laid end to end along the dimension named above; an argument that names none is the same for every part. Nothing has to cross between parts.
Inputs may be any that keep to these rules, and one draw needn't show every extreme that they name: Each part's 80 lengths sum to 81920, and the largest is exactly 4096.
All inputs are finite; a program needn't handle non-finite values.
Results may differ from a plain program's by a relative error of at most 0.018.
Values may be sent and summed in bfloat16 or wider, within the bound.
A program may use at most 128 MiB of HBM per device.

v0:
```python
import jax
import jax.numpy as jnp
from jax import lax
from jax.sharding import PartitionSpec as P

HEADS = 8
HEAD = 256
MAXLEN = 4096


EPS = 1e-05


def from_partner(value, axis, stride):
    mask = 2**stride
    pairs = [(source, source ^ mask) for source in range(lax.axis_size(axis))]
    return lax.ppermute(value, axis, pairs)


def body(
    tokens,
    lengths,
    cell_memory,
    key_sums,
    stabilizer,
    norm_gain,
    query_weight,
    key_weight,
    value_weight,
    outgate_weight,
    ingate_weight,
    forget_weight,
    ingate_bias,
    forget_bias,
    forget_slope,
    head_gain,
    output_weight,
):
    devices = lax.axis_size("tp")
    split_count = devices // HEADS
    own_index = lax.axis_index("tp")
    head_id = own_index // split_count
    onehot = (jnp.arange(HEADS) == head_id).astype(jnp.float32)
    position = lengths.astype(jnp.float32) / MAXLEN
    current = tokens
    memories, sums_list, stabs = ([], [], [])
    for block_id in range(cell_memory.shape[0]):
        gathered_rows = lax.all_gather(current, "tp", axis=1, tiled=True)
        row_float = gathered_rows.astype(jnp.float32)
        normed = (
            row_float
            * lax.rsqrt(jnp.mean(row_float * row_float, axis=-1, keepdims=True) + EPS)
            * norm_gain[block_id].astype(jnp.float32)
        ).astype(jnp.bfloat16)
        queries = jnp.dot(
            normed, query_weight[block_id], preferred_element_type=jnp.float32
        ).astype(jnp.bfloat16)
        key_rows = (
            jnp.dot(normed, key_weight[block_id], preferred_element_type=jnp.float32)
            * HEAD ** (-0.5)
        ).astype(jnp.bfloat16)
        values = jnp.dot(normed, value_weight[block_id], preferred_element_type=jnp.float32).astype(
            jnp.bfloat16
        )
        outgate = jnp.dot(
            normed, outgate_weight[block_id], preferred_element_type=jnp.float32
        ).astype(jnp.bfloat16)
        ingate = (
            jnp.dot(normed, ingate_weight[block_id], preferred_element_type=jnp.float32)
            + ingate_bias[block_id]
        )
        forget = jax.nn.log_sigmoid(
            jnp.dot(normed, forget_weight[block_id], preferred_element_type=jnp.float32)
            + forget_bias[block_id]
            + forget_slope[block_id] * position[:, None]
        )
        stab_new = jnp.maximum(forget + stabilizer[block_id], ingate)
        decays = jnp.exp(forget + stabilizer[block_id] - stab_new)
        in_weight = jnp.exp(ingate - stab_new)
        decay_own = jnp.sum(decays * onehot, axis=1)
        inweight_own = jnp.sum(in_weight * onehot, axis=1)
        sums_new = decay_own[:, None] * key_sums[block_id] + inweight_own[
            :, None
        ] * key_rows.astype(jnp.float32)
        head_pair = jnp.stack((queries, key_rows))
        head_sums = sums_new
        for level in range(split_count.bit_length() - 1):
            partner = from_partner(head_pair, "tp", level)
            upper = own_index // (1 << level) % 2 == 1
            lower_half = jnp.where(upper, partner, head_pair)
            upper_half = jnp.where(upper, head_pair, partner)
            head_pair = jnp.concatenate((lower_half, upper_half), axis=2)
            sums_mate = from_partner(head_sums, "tp", level)
            sums_low = jnp.where(upper, sums_mate, head_sums)
            sums_high = jnp.where(upper, head_sums, sums_mate)
            head_sums = jnp.concatenate((sums_low, sums_high), axis=1)
        head_query = head_pair[0].astype(jnp.float32)
        head_keys = head_pair[1].astype(jnp.float32)
        mem_new = (
            decay_own[:, None, None] * cell_memory[block_id]
            + inweight_own[:, None, None]
            * values.astype(jnp.float32)[:, :, None]
            * head_keys[:, None, :]
        )
        numerator = jnp.einsum("bvk,bk->bv", mem_new, head_query, precision=lax.Precision.HIGHEST)
        denominator = jnp.maximum(jnp.abs(jnp.sum(head_sums * head_query, axis=1)), 1.0)
        hidden = numerator / denominator[:, None]
        gated_out = (
            hidden
            * head_gain[block_id].astype(jnp.float32)
            * jax.nn.sigmoid(outgate.astype(jnp.float32))
        ).astype(jnp.bfloat16)
        out_weight = output_weight[block_id]
        projected = jnp.dot(
            lax.all_gather(gated_out, "tp", axis=1, tiled=True),
            out_weight,
            preferred_element_type=jnp.float32,
        )
        current = (current.astype(jnp.float32) + projected).astype(jnp.bfloat16)
        memories.append(mem_new)
        sums_list.append(sums_new)
        stabs.append(stab_new)
    return (current, jnp.stack(memories), jnp.stack(sums_list), jnp.stack(stabs))


def solution(mesh):
    in_specs = (
        P("grp", "tp"),
        P("grp"),
        P(None, "grp", "tp", None),
        P(None, "grp", "tp"),
        P(None, "grp", None),
        P(),
        P(None, None, "tp"),
        P(None, None, "tp"),
        P(None, None, "tp"),
        P(None, None, "tp"),
        P(),
        P(),
        P(),
        P(),
        P(),
        P(None, "tp"),
        P(None, None, "tp"),
    )
    out_specs = (
        P("grp", "tp"),
        P(None, "grp", "tp", None),
        P(None, "grp", "tp"),
        P(None, "grp", None),
    )
    return jax.shard_map(body, mesh=mesh, in_specs=in_specs, out_specs=out_specs, check_vma=False)
```

profile of v0, /device:TPU:1, one launch (start us, length us, event | category | flops | bytes accessed | tf_op | source)
XLA Modules:
  0.0 133.3 jit_solution(18110746305476406706)
XLA Ops:
  0.7 0.7 convert_multiply_fusion.4
  1.3 0.8 slice_bitcast_fusion
  2.1 0.8 slice_convert_fusion
  2.9 24.1 %all_gather.12 = bf16[80,2048]{1,0:T(8,128)(2,1)S(1)} all-gather(bf16[80,128]{1,0:T(8,128)(2,1)} %param.17), channel_id=1, replica_groups=mesh['grp'=2,'tp'=16] {'tp'}, dimensions={1}, use_global_device_ids=true | all-gather | bytes 348160 | tf_op jit(solution)/shard_map/all_gather | solution.py:48
  27.2 0.8 slice_bitcast_fusion.1
  27.9 1.3 %fusion.38 = bf16[1,80,128]{2,1,0:T(8,128)(2,1)S(1)} fusion(bf16[2,2048,128]{2,1,0:T(8,128)(2,1)} %param.23, bf16[80,2048]{1,0:T(8,128)(2,1)S(1)} %all_gather.12, f32[2048]{0:T(1024)S(1)} %bitcast.144, f32[80]{0:T(128)S(1)} %add_rsqrt_fusion.1), kind=kOutput, calls=%fused_computation.51 | convolution fusion | flops 42608640 | bytes 880960 | tf_op jit(solution)/shard_map/dot_general | solution.py:55
  29.3 1.1 fusion.93
  30.4 1.1 multiply_reduce_fusion.3
  31.5 1.4 %fusion.81 = (f32[80,128]{1,0:T(8,128)S(1)}, bf16[80,128]{1,0:T(8,128)(2,1)S(1)}) fusion(f32[2,80,128]{2,1,0:T(8,128)} %param.20, f32[80]{0:T(128)S(1)} %get-tuple-element.6, f32[80]{0:T(128)S(1)} %get-tuple-element.7, bf16[2,2048,128]{2,1,0:T(8,128)(2,1)} %param.24, bf16[80,2048]{1,0:T(8,128)(2,1)S(1)} %all_gather.12, f32[2048]{0:T(1024)S(1)} %bitcast.147, ...), kind=kOutput, calls=%fused_computation.115 | convolution fusion | flops 42659840 | bytes 963520 | tf_op jit(solution)/shard_map/dot_general | solution.py:59
  32.9 0.2 collective-permute-start
  33.2 0.3 collective-permute-start.1
  33.5 1.3 %fusion.37 = f32[80,128]{1,0:T(8,128)S(1)} fusion(bf16[2,2048,128]{2,1,0:T(8,128)(2,1)} %param.25, f32[80]{0:T(128)S(1)} %get-tuple-element.7, bf16[80,2048]{1,0:T(8,128)(2,1)S(1)} %all_gather.12, f32[2048]{0:T(1024)S(1)} %bitcast.148, f32[80]{0:T(128)S(1)} %add_rsqrt_fusion.1), kind=kOutput, calls=%fused_computation.50 | convolution fusion | flops 42629120 | bytes 901760 | tf_op jit(solution)/shard_map/dot_general | solution.py:62
  34.9 0.7 bitcast_convert_fusion
  35.8 8.7 %fusion.4 = f32[80,1,128]{2,1,0:T(1,128)S(1)} fusion(f32[2,80,128,256]{3,2,1,0:T(8,128)} %param.19, f32[80,256]{1,0:T(8,128)S(1)} %get-tuple-element.19, f32[80,128]{1,0:T(8,128)S(1)} %fusion.37, f32[80]{0:T(128)S(1)} %get-tuple-element.6, bf16[80,256,1]{1,0,2:T(8,128)(2,1)S(1)} %get-tuple-element.18), kind=kOutput, calls=%fused_computation.6 | convolution fusion | flops 39321600 | bytes 10690880 | tf_op jit(solution)/shard_map/bvk,bk->bv/dot_general | solution.py:105
  44.5 0.3 fusion.35
  44.9 18.3 %all_gather.13 = bf16[80,2048]{1,0:T(8,128)(2,1)S(1)} all-gather(bf16[80,128]{1,0:T(8,128)(2,1)S(1)} %fusion.35), channel_id=1, replica_groups=mesh['grp'=2,'tp'=16] {'tp'}, dimensions={1}, use_global_device_ids=true | all-gather | bytes 348160 | tf_op jit(solution)/shard_map/all_gather | solution.py:115
  63.2 0.2 fusion.17
  63.5 19.7 %all_gather.14 = bf16[80,2048]{1,0:T(8,128)(2,1)S(1)} all-gather(bf16[80,128]{1,0:T(8,128)(2,1)S(1)} %fusion.17), channel_id=1, replica_groups=mesh['grp'=2,'tp'=16] {'tp'}, dimensions={1}, use_global_device_ids=true | all-gather | bytes 348160 | tf_op jit(solution)/shard_map/all_gather | solution.py:48
  83.3 0.3 fusion.39
  83.6 0.3 fusion.95
  83.9 0.3 multiply_reduce_fusion.1
  84.2 0.3 fusion.28
  84.6 0.3 fusion.80
  85.1 0.3 collective-permute-start.3
  85.5 0.6 pad_maximum_fusion.1
  86.1 0.6 pad_maximum_fusion.6
  86.9 10.3 %multiply_add_fusion.1 = (f32[1,80,128,256]{3,2,1,0:T(8,128)S(1)}, f32[1,80,128,256]{3,2,1,0:T(8,128)S(1)}) fusion(f32[2,80,128,256]{3,2,1,0:T(8,128)} %param.19, f32[80,256]{1,0:T(8,128)S(1)} %get-tuple-element.19, f32[80,128]{1,0:T(8,128)S(1)} %fusion.37, f32[80]{0:T(128)S(1)} %get-tuple-element.6, f32[80,256]{1,0:T(8,128)S(1)} %get-tuple-element.13, ...), kind=kLoop, calls=%fused_computation.8 | loop fusion | flops 15728640 | bytes 42189440 | tf_op jit(solution)/shard_map/add | solution.py:100
  97.3 8.6 %fusion.1 = f32[80,1,128]{2,1,0:T(1,128)S(1)} fusion(f32[2,80,128,256]{3,2,1,0:T(8,128)} %param.19, f32[80,256]{1,0:T(8,128)S(1)} %get-tuple-element.13, f32[80,128]{1,0:T(8,128)S(1)} %fusion.28, f32[80]{0:T(128)S(1)} %get-tuple-element.4, bf16[80,256,1]{1,0,2:T(8,128)(2,1)S(1)} %get-tuple-element.12), kind=kOutput, calls=%fused_computation.3 | convolution fusion | flops 39321600 | bytes 10690880 | tf_op jit(solution)/shard_map/bvk,bk->bv/dot_general | solution.py:105
  105.8 0.3 fusion.26
  106.1 18.3 %all_gather.15 = bf16[80,2048]{1,0:T(8,128)(2,1)S(1)} all-gather(bf16[80,128]{1,0:T(8,128)(2,1)S(1)} %fusion.26), channel_id=1, replica_groups=mesh['grp'=2,'tp'=16] {'tp'}, dimensions={1}, use_global_device_ids=true | all-gather | bytes 348160 | tf_op jit(solution)/shard_map/all_gather | solution.py:115
  124.5 0.9 fusion.19
  125.3 8.0 %pad_maximum_fusion = f32[2,80,128,256]{3,2,1,0:T(8,128)} fusion(f32[1,80,128,256]{3,2,1,0:T(8,128)S(1)} %get-tuple-element.9, f32[1,80,128,256]{3,2,1,0:T(8,128)S(1)} %get-tuple-element.8), kind=kLoop, calls=%fused_computation | loop fusion | flops 5242880 | bytes 41943040 | tf_op jit(solution)/shard_map/stack | solution.py:123
  (42 shorter events, 0.9 us)
Async XLA Ops:
  27.0 36.2 %copy-start = (bf16[80,128]{1,0:T(8,128)(2,1)S(1)}, bf16[80,128]{1,0:T(8,128)(2,1)}, u32[]{:S(2)}) copy-start(bf16[80,128]{1,0:T(8,128)(2,1)} %param.17) | copy-start | bytes 61444
  29.3 54.0 %copy-start.1 = (bf16[2,2048,128]{2,1,0:T(8,128)(2,1)S(1)}, bf16[2,2048,128]{2,1,0:T(8,128)(2,1)}, u32[]{:S(2)}) copy-start(bf16[2,2048,128]{2,1,0:T(8,128)(2,1)} %param.23) | copy-start | bytes 3145732
  31.5 52.1 %copy-start.7 = (bf16[2,2048,8]{1,2,0:T(8,128)(2,1)S(1)}, bf16[2,2048,8]{1,2,0:T(8,128)(2,1)}, u32[]{:S(2)}) copy-start(bf16[2,2048,8]{1,2,0:T(8,128)(2,1)} %param.28) | copy-start | bytes 196612
  31.5 52.1 %copy-start.9 = (f32[2,80,8]{1,2,0:T(8,128)S(1)}, f32[2,80,8]{1,2,0:T(8,128)}, u32[]{:S(2)}) copy-start(f32[2,80,8]{1,2,0:T(8,128)} %param.21) | copy-start | bytes 15364
  31.5 52.4 %copy-start.8 = (bf16[2,2048,8]{1,2,0:T(8,128)(2,1)S(1)}, bf16[2,2048,8]{1,2,0:T(8,128)(2,1)}, u32[]{:S(2)}) copy-start(bf16[2,2048,8]{1,2,0:T(8,128)(2,1)} %param.27) | copy-start | bytes 196612
  32.9 51.3 %copy-start.2 = (bf16[2,2048,128]{2,1,0:T(8,128)(2,1)S(1)}, bf16[2,2048,128]{2,1,0:T(8,128)(2,1)}, u32[]{:S(2)}) copy-start(bf16[2,2048,128]{2,1,0:T(8,128)(2,1)} %param.25) | copy-start | bytes 3145732
  32.9 2.7 %collective-permute-start = (bf16[2,80,128]{2,1,0:T(8,128)(2,1)S(1)}, bf16[2,80,128]{2,1,0:T(8,128)(2,1)S(1)}, u32[]{:S(2)}, u32[]{:S(2)}) collective-permute-start(bf16[2,80,128]{2,1,0:T(8,128)(2,1)S(1)} %pad_maximum_fusion.4), channel_id=1, source_target_pairs={{0,1},{1,0},{2,3},{3,2},{4,5},{5,4},{6,7},{7,6},{8,9},{9,8},{10,11... | collective-permute-start | bytes 122888 | tf_op jit(solution)/shard_map/ppermute | solution.py:17
  33.2 2.5 %collective-permute-start.1 = (f32[80,128]{1,0:T(8,128)S(1)}, f32[80,128]{1,0:T(8,128)S(1)}, u32[]{:S(2)}, u32[]{:S(2)}) collective-permute-start(f32[80,128]{1,0:T(8,128)S(1)} %get-tuple-element.34), channel_id=1, source_target_pairs={{0,1},{1,0},{2,3},{3,2},{4,5},{5,4},{6,7},{7,6},{8,9},{9,8},{10,11... | collective-permute-start | bytes 122888 | tf_op jit(solution)/shard_map/ppermute | solution.py:17
  34.9 49.7 %copy-start.6 = (f32[2,80,128]{2,1,0:T(8,128)S(1)}, f32[2,80,128]{2,1,0:T(8,128)}, u32[]{:S(2)}) copy-start(f32[2,80,128]{2,1,0:T(8,128)} %param.20) | copy-start | bytes 245764
  35.6 8.9 %copy-start.4 = (bf16[2,2048,128]{2,1,0:T(8,128)(2,1)S(1)}, bf16[2,2048,128]{2,1,0:T(8,128)(2,1)}, u32[]{:S(2)}) copy-start(bf16[2,2048,128]{2,1,0:T(8,128)(2,1)} %param.26) | copy-start | bytes 3145732
  35.6 27.6 %copy-start.5 = (bf16[2,2048,128]{2,1,0:T(8,128)(2,1)S(1)}, bf16[2,2048,128]{2,1,0:T(8,128)(2,1)}, u32[]{:S(2)}) copy-start(bf16[2,2048,128]{2,1,0:T(8,128)(2,1)} %param.33) | copy-start | bytes 3145732
  35.6 48.9 %copy-start.3 = (bf16[2,2048,128]{2,1,0:T(8,128)(2,1)S(1)}, bf16[2,2048,128]{2,1,0:T(8,128)(2,1)}, u32[]{:S(2)}) copy-start(bf16[2,2048,128]{2,1,0:T(8,128)(2,1)} %param.24) | copy-start | bytes 3145732
  84.9 1.8 %collective-permute-start.2 = (bf16[2,80,128]{2,1,0:T(8,128)(2,1)S(1)}, bf16[2,80,128]{2,1,0:T(8,128)(2,1)S(1)}, u32[]{:S(2)}, u32[]{:S(2)}) collective-permute-start(bf16[2,80,128]{2,1,0:T(8,128)(2,1)S(1)} %pad_maximum_fusion.5), channel_id=1, source_target_pairs={{0,1},{1,0},{2,3},{3,2},{4,5},{5,4},{6,7},{7,6},{8,9},{9,8},{10,11... | collective-permute-start | bytes 122888 | tf_op jit(solution)/shard_map/ppermute | solution.py:17
  85.1 1.6 %collective-permute-start.3 = (f32[80,128]{1,0:T(8,128)S(1)}, f32[80,128]{1,0:T(8,128)S(1)}, u32[]{:S(2)}, u32[]{:S(2)}) collective-permute-start(f32[80,128]{1,0:T(8,128)S(1)} %get-tuple-element.36), channel_id=1, source_target_pairs={{0,1},{1,0},{2,3},{3,2},{4,5},{5,4},{6,7},{7,6},{8,9},{9,8},{10,11... | collective-permute-start | bytes 122888 | tf_op jit(solution)/shard_map/ppermute | solution.py:17
where the time goes:
time: 134 us; the launch traced here: 133 us
  blocking collectives  80.4 us (60%)
  matrix products  26.8 us (20%)
  other arithmetic  22.4 us (17%)
  local copies, waits for them, and re-layouts  1.58 us (1%)
    all_gather x2, blocking collectives, body(): gathered_rows = lax.all_gather(current, 'tp', axis=1, tiled=True)  43.8 us
    all_gather x2, blocking collectives, body(): lax.all_gather(gated_out, 'tp', axis=1, tiled=True)  36.7 us
    dot_general x2, matrix products, body(): jnp.einsum('bvk,bk->bv', mem_new, head_query, precision=lax.Precision.HIG...  17.2 us
    add x1, other arithmetic, body(): decay_own[:, None, None] * cell_memory[block_id]  10.3 us
    another operation x1, other arithmetic, body(): jnp.stack(memories)  8 us
  transfers between devices with their start and end apart: 4, of which 0 were waited for; matrix products, arithmetic and copies ran while one was open for 3% of the time, Pallas kernels for 0%

commit v1 on v0

--- a/solution.py
+++ b/solution.py
@@ -1,14 +1,327 @@
+import functools
+
 import jax
 import jax.numpy as jnp
 from jax import lax
+from jax.experimental import pallas as pl
+from jax.experimental.pallas import tpu as pltpu
 from jax.sharding import PartitionSpec as P
 
 HEADS = 8
 HEAD = 256
 MAXLEN = 4096
-
-
 EPS = 1e-05
+MESH = pl.DeviceIdType.MESH
+F32 = jnp.float32
+BF16 = jnp.bfloat16
+GROUP = 8
+
+
+def kernel(
+    n,
+    tokens,
+    lengths,
+    cell_memory,
+    key_sums,
+    stabilizer,
+    norm_gain,
+    query_weight,
+    key_weight,
+    value_weight,
+    outgate_weight,
+    ingate_weight,
+    forget_weight,
+    ingate_bias,
+    forget_bias,
+    forget_slope,
+    head_gain,
+    output_weight,
+    new_tokens,
+    mem,
+    new_sums,
+    new_stab,
+    lengths_in,
+    stabilizer_in,
+    norm_gain_in,
+    ingate_bias_in,
+    forget_bias_in,
+    forget_slope_in,
+    head_gain_in,
+    wbig,
+    wout,
+    wgi,
+    wgf,
+    wgate,
+    small_sem,
+    gath,
+    pair,
+    sums,
+    vt_ref,
+    decay_ref,
+    kk_ref,
+    local_sem,
+    mem_sem,
+    gsend,
+    gfwd,
+    grecv,
+    psend,
+    precv,
+    ssend,
+    srecv,
+):
+    blocks, batch, rows, head = mem.shape
+    heads = stabilizer.shape[1]
+    width = output_weight.shape[1]
+    split = n // heads
+    chips = n // 2
+    me = lax.axis_index("tp")
+    chip = me // 2
+    core = lax.rem(me, 2)
+    sibling = me + 1 - 2 * core
+    own_head = me // split
+    lanes = pl.multiple_of
+
+    def target(j):
+        return lax.rem(chip + j, chips) * 2 + core
+
+    def source(j):
+        return lax.rem(chip + chips - j, chips) * 2 + core
+
+    own_copy = pltpu.make_async_copy(tokens, gath.at[0, me], local_sem.at[0, 7])
+    own_copy.start()
+    sums_copy = pltpu.make_async_copy(key_sums, sums.at[core], local_sem.at[1, 7])
+    sums_copy.start()
+    small = [
+        pltpu.make_async_copy(a, b, small_sem.at[i])
+        for i, (a, b) in enumerate(
+            (
+                (lengths, lengths_in),
+                (stabilizer, stabilizer_in),
+                (norm_gain, norm_gain_in),
+                (ingate_bias, ingate_bias_in),
+                (forget_bias, forget_bias_in),
+                (forget_slope, forget_slope_in),
+                (head_gain, head_gain_in),
+            )
+        )
+    ]
+    for c in small:
+        c.start()
+    wcopies, mcopies = [], []
+    for l in range(blocks):
+        now = []
+        for i, w in enumerate((query_weight, key_weight, value_weight, outgate_weight)):
+            now.append(
+                pltpu.make_async_copy(
+                    w.at[l], wbig.at[l, :, pl.ds(i * rows, rows)], local_sem.at[l, i]
+                )
+            )
+        now.append(pltpu.make_async_copy(ingate_weight.at[l], wgi.at[l], local_sem.at[l, 4]))
+        now.append(pltpu.make_async_copy(forget_weight.at[l], wgf.at[l], local_sem.at[l, 5]))
+        now.append(pltpu.make_async_copy(output_weight.at[l], wout.at[l], local_sem.at[l, 6]))
+        wcopies.append(now)
+        mcopies.append(pltpu.make_async_copy(cell_memory.at[l], mem.at[l], mem_sem.at[l]))
+        for c in now:
+            c.start()
+        mcopies[l].start()
+
+    barrier = pltpu.get_barrier_semaphore()
+    pl.semaphore_signal(barrier, inc=1, device_id={"tp": sibling}, device_id_type=MESH)
+    for j in range(1, chips):
+        pl.semaphore_signal(barrier, inc=1, device_id={"tp": target(j)}, device_id_type=MESH)
+    pl.semaphore_wait(barrier, chips)
+
+    def block_copy(g, slot, sems, k, dest):
+        return pltpu.make_async_remote_copy(
+            src_ref=gath.at[g, slot],
+            dst_ref=gath.at[g, slot],
+            send_sem=sems.at[g, k],
+            recv_sem=grecv.at[g, slot],
+            device_id={"tp": dest},
+            device_id_type=MESH,
+        )
+
+    sent = []
+
+    def send_own(g):
+        for j in range(1, chips):
+            c = block_copy(g, me, gsend, j, target(j))
+            c.start()
+            sent.append(c)
+        c = block_copy(g, me, gsend, 0, sibling)
+        c.start()
+        sent.append(c)
+
+    def arrive(g, step):
+        total = None
+        block_copy(g, sibling, gsend, 0, sibling).wait_recv()
+        total = step(chip, total)
+        for j in range(1, chips):
+            s = source(j)
+            block_copy(g, s, gsend, j, sibling).wait_recv()
+            c = block_copy(g, s, gfwd, j, sibling)
+            c.start()
+            sent.append(c)
+        for j in range(1, chips):
+            s = source(j)
+            block_copy(g, s + 1 - 2 * core, gsend, j, sibling).wait_recv()
+            total = step(s // 2, total)
+        return total
+
+    own_copy.wait()
+    send_own(0)
+    sums_copy.wait()
+    sums_send = pltpu.make_async_remote_copy(
+        src_ref=sums.at[core],
+        dst_ref=sums.at[core],
+        send_sem=ssend,
+        recv_sem=srecv,
+        device_id={"tp": sibling},
+        device_id_type=MESH,
+    )
+    sums_send.start()
+
+    for c in small:
+        c.wait()
+    eye = lax.broadcasted_iota(jnp.int32, (batch, batch), 0) == lax.broadcasted_iota(
+        jnp.int32, (batch, batch), 1
+    )
+    position = jnp.sum(
+        jnp.where(eye, lengths_in[...].astype(F32) / MAXLEN, 0.0), axis=1, keepdims=True
+    )
+    head_mask = lax.broadcasted_iota(jnp.int32, (batch, heads), 1) == own_head
+    current = gath[0, me].astype(F32)
+
+    for l in range(blocks):
+        for c in wcopies[l][:6]:
+            c.wait()
+        wgate[l] = jnp.concatenate((wgi[l].astype(F32), wgf[l].astype(F32)), axis=0).astype(BF16)
+        old_stab = stabilizer_in[l].T
+
+        def project(c, total, l=l):
+            at = pl.ds(lanes(c * 2 * rows, 2 * rows), 2 * rows)
+            x = jnp.concatenate((gath[2 * l, 2 * c], gath[2 * l, 2 * c + 1]), axis=1).astype(F32)
+            gain = norm_gain_in[:, at].astype(F32)[l : l + 1]
+            scaled = (x * gain).astype(BF16)
+            part = jnp.dot(scaled, wbig[l, at, :], preferred_element_type=F32)
+            gpart = lax.dot_general(
+                scaled, wgate[l, :, at], (((1,), (1,)), ((), ())), preferred_element_type=F32
+            )
+            square = x * x
+            if total is None:
+                return part, gpart, square
+            return total[0] + part, total[1] + gpart, total[2] + square
+
+        proj, gates, square = arrive(2 * l, project)
+        scale = lax.rsqrt(jnp.sum(square, axis=1, keepdims=True) / width + EPS)
+        proj = proj * scale
+        query = proj[:, :rows].astype(BF16)
+        keyrow = (proj[:, rows : 2 * rows] * head ** (-0.5)).astype(BF16)
+        pair[l, core, 0] = query
+        pair[l, core, 1] = keyrow
+        pair_send = pltpu.make_async_remote_copy(
+            src_ref=pair.at[l, core],
+            dst_ref=pair.at[l, core],
+            send_sem=psend.at[l],
+            recv_sem=precv.at[l],
+            device_id={"tp": sibling},
+            device_id_type=MESH,
+        )
+        pair_send.start()
+        value = proj[:, 2 * rows : 3 * rows].astype(BF16).astype(F32)
+        outgate = proj[:, 3 * rows : 4 * rows].astype(BF16).astype(F32)
+        gates = gates * scale
+        ingate = gates[:, :heads] + ingate_bias_in[l : l + 1, :]
+        logit = (
+            gates[:, heads : 2 * heads]
+            + forget_bias_in[l : l + 1, :]
+            + forget_slope_in[l : l + 1, :] * position
+        )
+        forget = jnp.minimum(logit, 0.0) - jnp.log1p(jnp.exp(-jnp.abs(logit)))
+        shifted = forget + old_stab
+        stab = jnp.maximum(shifted, ingate)
+        decay = jnp.sum(
+            jnp.where(head_mask, jnp.exp(shifted - stab), 0.0), axis=1, keepdims=True
+        )
+        inweight = jnp.sum(
+            jnp.where(head_mask, jnp.exp(ingate - stab), 0.0), axis=1, keepdims=True
+        )
+        new_sums[l] = decay * sums[core, l] + inweight * keyrow.astype(F32)
+        vt_ref[...] = jnp.concatenate((value, jnp.zeros((rows - batch, rows), F32)), axis=0).T
+        decay_ref[...] = jnp.broadcast_to(decay, (batch, head))
+        gate = (
+            head_gain_in[...].astype(F32)[l : l + 1] * jax.nn.sigmoid(outgate)
+        )
+
+        pair_send.wait_send()
+        sib_pair = pltpu.make_async_remote_copy(
+            src_ref=pair.at[l, 1 - core],
+            dst_ref=pair.at[l, 1 - core],
+            send_sem=psend.at[l],
+            recv_sem=precv.at[l],
+            device_id={"tp": sibling},
+            device_id_type=MESH,
+        )
+        sib_pair.wait_recv()
+        if l == 0:
+            sums_send.wait()
+        head_query = jnp.concatenate((pair[l, 0, 0], pair[l, 1, 0]), axis=1)
+        head_key = jnp.concatenate((pair[l, 0, 1], pair[l, 1, 1]), axis=1).astype(F32)
+        query_float = head_query.astype(F32)
+        kk_ref[...] = inweight * head_key
+        key_dot = jnp.sum(head_key * query_float, axis=1, keepdims=True)
+        old = jnp.concatenate((sums[0, l], sums[1, l]), axis=1)
+        sum_dot = jnp.sum(old * query_float, axis=1, keepdims=True)
+        denominator = jnp.maximum(jnp.abs(decay * sum_dot + inweight * key_dot), 1.0)
+        padded = jnp.concatenate((head_query, jnp.zeros((rows - batch, head), BF16)), axis=0)
+
+        mcopies[l].wait()
+        lane = lax.broadcasted_iota(jnp.int32, (rows, rows), 1)
+
+        def read(g, acc, l=l, padded=padded, lane=lane):
+            at = g * GROUP
+            c = mem[l, pl.ds(at, GROUP)].reshape(GROUP * rows, head).astype(BF16)
+            r = lax.dot_general(
+                c, padded, (((1,), (1,)), ((), ())), preferred_element_type=F32
+            ).reshape(GROUP, rows, rows)
+            for i in range(GROUP):
+                acc = jnp.where(lane == at + i, r[i], acc)
+            return acc
+
+        readout = lax.fori_loop(0, batch // GROUP, read, jnp.zeros((rows, rows), F32)).T[:batch]
+        hidden = (decay * readout + (inweight * key_dot) * value) / denominator
+        gath[2 * l + 1, me] = (hidden * gate).astype(BF16)
+        send_own(2 * l + 1)
+        new_stab[l] = stab.T
+
+        @pl.loop(0, batch // GROUP)
+        def _(g, l=l):
+            at = g * GROUP
+            v = pltpu.roll(vt_ref[...], lax.rem(rows - at, rows), 1)
+            for i in range(GROUP):
+                mem[l, at + i] = mem[l, at + i] * decay_ref[pl.ds(at + i, 1), :] + v[
+                    :, i : i + 1
+                ] * kk_ref[pl.ds(at + i, 1), :]
+
+        wcopies[l][6].wait()
+
+        def output(c, total, l=l):
+            at = pl.ds(lanes(c * 2 * rows, 2 * rows), 2 * rows)
+            x = jnp.concatenate((gath[2 * l + 1, 2 * c], gath[2 * l + 1, 2 * c + 1]), axis=1)
+            part = jnp.dot(x, wout[l, at, :], preferred_element_type=F32)
+            return part if total is None else total + part
+
+        moved = arrive(2 * l + 1, output)
+        nxt = (current + moved).astype(BF16)
+        current = nxt.astype(F32)
+        if l + 1 < blocks:
+            gath[2 * l + 2, me] = nxt
+            send_own(2 * l + 2)
+        else:
+            new_tokens[...] = nxt
+
+    for c in sent:
+        c.wait_send()
 
 
 def from_partner(value, axis, stride):
@@ -17,7 +330,7 @@
     return lax.ppermute(value, axis, pairs)
 
 
-def body(
+def plain_body(
     tokens,
     lengths,
     cell_memory,
@@ -123,6 +436,92 @@
     return (current, jnp.stack(memories), jnp.stack(sums_list), jnp.stack(stabs))
 
 
+def write_out(*refs):
+    sems = refs[8]
+    copies = [pltpu.make_async_copy(refs[i], refs[4 + i], sems.at[i]) for i in range(4)]
+    for c in copies:
+        c.start()
+    for c in copies:
+        c.wait()
+
+
+def body(*args):
+    tokens, lengths, cell_memory, key_sums, stabilizer = args[:5]
+    n = lax.axis_size("tp")
+    blocks, batch, rows, head = cell_memory.shape
+    heads = stabilizer.shape[2]
+    width = args[6].shape[1]
+    if n != 2 * heads or rows < batch or rows % 128 or batch % GROUP:
+        return plain_body(*args)
+    vm = pl.BlockSpec(memory_space=pltpu.VMEM)
+    anyspace = pl.BlockSpec(memory_space=pl.ANY)
+    dma = pltpu.SemaphoreType.DMA
+    in_specs = [pl.BlockSpec(memory_space=pltpu.HBM)] * 17
+    results = pl.pallas_call(
+        functools.partial(kernel, n),
+        out_shape=(
+            pltpu.VMEM((batch, rows), BF16),
+            pltpu.VMEM(cell_memory.shape, F32),
+            pltpu.VMEM(key_sums.shape, F32),
+            pltpu.VMEM((blocks, heads, batch), F32),
+        ),
+        in_specs=in_specs,
+        out_specs=(vm, vm, vm, vm),
+        scratch_shapes=[
+            pltpu.VMEM((1, batch), jnp.int32),
+            pltpu.VMEM((blocks, heads, batch), F32),
+            pltpu.VMEM((blocks, width), BF16),
+            pltpu.VMEM((blocks, heads), F32),
+            pltpu.VMEM((blocks, heads), F32),
+            pltpu.VMEM((blocks, heads), F32),
+            pltpu.VMEM((blocks, rows), BF16),
+            pltpu.VMEM((blocks, width, 4 * rows), BF16),
+            pltpu.VMEM((blocks, width, rows), BF16),
+            pltpu.VMEM((blocks, heads, width), BF16),
+            pltpu.VMEM((blocks, heads, width), BF16),
+            pltpu.VMEM((blocks, 2 * heads, width), BF16),
+            dma((7,)),
+            pltpu.VMEM((2 * blocks, n, batch, rows), BF16),
+            pltpu.VMEM((blocks, 2, 2, batch, rows), BF16),
+            pltpu.VMEM((2, blocks, batch, rows), F32),
+            pltpu.VMEM((rows, rows), F32),
+            pltpu.VMEM((batch, head), F32),
+            pltpu.VMEM((batch, head), F32),
+            dma((blocks, 8)),
+            dma((blocks,)),
+            dma((2 * blocks, n // 2)),
+            dma((2 * blocks, n // 2)),
+            dma((2 * blocks, n)),
+            dma((blocks,)),
+            dma((blocks,)),
+            dma,
+            dma,
+        ],
+        compiler_params=pltpu.CompilerParams(
+            collective_id=0, has_side_effects=True, vmem_limit_bytes=45500000
+        ),
+    )(
+        tokens,
+        lengths.reshape(1, batch),
+        cell_memory,
+        key_sums,
+        stabilizer.swapaxes(1, 2),
+        *args[5:10],
+        args[10].swapaxes(1, 2),
+        args[11].swapaxes(1, 2),
+        *args[12:],
+    )
+    final = pl.pallas_call(
+        write_out,
+        out_shape=tuple(jax.ShapeDtypeStruct(r.shape, r.dtype) for r in results),
+        in_specs=[anyspace] * 4,
+        out_specs=(anyspace,) * 4,
+        scratch_shapes=[dma((4,))],
+        compiler_params=pltpu.CompilerParams(vmem_limit_bytes=1024 * 1024),
+    )(*results)
+    return (*final[:3], final[3].swapaxes(1, 2))
+
+
 def solution(mesh):
     in_specs = (
         P("grp", "tp"),

time: 134 us -> 51.3 us (0.38)
  blocking collectives: 80.4 us -> 0 us
  Pallas kernels: 0 us -> 50.5 us
  matrix products: 26.8 us -> 0 us
  other arithmetic: 22.4 us -> 0 us
  local copies, waits for them, and re-layouts: 1.58 us -> 0 us
    all_gather x4 -> x0, blocking collectives: 80.4 us -> none  [the longest x2 43.8 us: body(): gathered_rows = lax.all_gather(current, 'tp', axis=1, tiled=True)]
    pallas_call x0 -> x2, Pallas kernels: none -> 50.5 us  [the longest x1 42.9 us: body(): pl.pallas_call(functools.partial(kernel, n), out_shape=(pltpu.VMEM((batch...]
    dot_general x16 -> x0, matrix products: 26.8 us -> none  [the longest x2 17.2 us: body(): jnp.einsum('bvk,bk->bv', mem_new, head_query, precision=lax.Precision.HIG...]
    add x1 -> x0, other arithmetic: 10.3 us -> none  [body(): decay_own[:, None, None] * cell_memory[block_id]]
    another operation x5 -> x0, other arithmetic: 9.26 us -> none  [the longest x1 8 us: body(): jnp.stack(memories)]
    mul x2 -> x0, other arithmetic: 1.52 us -> none  [the longest x1 0.79 us: body(): row_float * lax.rsqrt(jnp.mean(row_float * row_float, axis=-1, keepdims=T...]
  transfers between devices with their start and end apart: 4 -> 0, of which waited for: 0 -> 0; matrix products, arithmetic and copies ran while one was open for 3% -> 0% of each run, Pallas kernels for 0% -> 0%
where the time goes in v1:
time: 51.3 us; the launch traced here: 51.1 us
  Pallas kernels  50.5 us (98%)
  between operations  0.65 us (1%)
    pallas_call x1, Pallas kernels, body(): pl.pallas_call(functools.partial(kernel, n), out_shape=(pltpu.VMEM((batch...  42.9 us
    pallas_call x1, Pallas kernels, body(): pl.pallas_call(write_out, out_shape=tuple((jax.ShapeDtypeStruct(r.shape,...  7.59 us

profile of v1, /device:TPU:1, one launch (start us, length us, event | category | flops | bytes accessed | tf_op | source)
XLA Modules:
  0.0 51.1 jit_solution(2521899802748201548)
XLA Ops:
  0.6 42.9 %shard_map.192 = (bf16[80,128]{1,0:T(8,128)(2,1)S(1)}, f32[2,80,128,256]{3,2,1,0:T(8,128)S(1)}, f32[2,80,128]{2,1,0:T(8,128)S(1)}, f32[2,8,80]{2,1,0:T(8,128)S(1)}) custom-call(bf16[80,128]{1,0:T(8,128)(2,1)} %tokens.1, s32[1,80]{1,0:T(1,128)} %bitcast.8, f32[2,80,128,256]{3,2,1,0:T(8,128)} %cell_memory.1, f32[2,80,128]{2,1,0:T(8,128)} %key_sums.1, ...), custom_call_target="tpu_custom_call" | custom-call | tf_op jit(solution)/shard_map/pallas_call | solution.py:460
  43.5 7.6 %shard_map.193 = (bf16[80,128]{1,0:T(8,128)(2,1)}, f32[2,80,128,256]{3,2,1,0:T(8,128)}, f32[2,80,128]{2,1,0:T(8,128)}, f32[2,8,80]{2,1,0:T(8,128)}) custom-call(bf16[80,128]{1,0:T(8,128)(2,1)S(1)} %get-tuple-element.12.refs_0_, f32[2,80,128,256]{3,2,1,0:T(8,128)S(1)} %get-tuple-element.13.refs_1_, f32[2,80,128]{2,1,0:T(8,128)S(1)} %get-tuple-element.14.refs_2_, ...), custom_call_target="tpu_custom_call" | custom-call | tf_op jit(solution)/shard_map/pallas_call | solution.py:514

commit v2 on v1

--- a/solution.py
+++ b/solution.py
@@ -288,7 +288,7 @@
                 acc = jnp.where(lane == at + i, r[i], acc)
             return acc
 
-        readout = lax.fori_loop(0, batch // GROUP, read, jnp.zeros((rows, rows), F32)).T[:batch]
+        readout = lax.fori_loop(0, batch // GROUP, read, jnp.zeros((rows, rows), F32), unroll=5).T[:batch]
         hidden = (decay * readout + (inweight * key_dot) * value) / denominator
         gath[2 * l + 1, me] = (hidden * gate).astype(BF16)
         send_own(2 * l + 1)
@@ -438,7 +438,16 @@
 
 def write_out(*refs):
     sems = refs[8]
-    copies = [pltpu.make_async_copy(refs[i], refs[4 + i], sems.at[i]) for i in range(4)]
+    copies = [pltpu.make_async_copy(refs[i], refs[4 + i], sems.at[i]) for i in (0, 2, 3)]
+    blocks, batch = refs[1].shape[:2]
+    for l in range(blocks):
+        for g in range(batch // GROUP):
+            at = pl.ds(g * GROUP, GROUP)
+            copies.append(
+                pltpu.make_async_copy(
+                    refs[1].at[l, at], refs[5].at[l, at], sems.at[4 + l * (batch // GROUP) + g]
+                )
+            )
     for c in copies:
         c.start()
     for c in copies:
@@ -516,7 +525,7 @@
         out_shape=tuple(jax.ShapeDtypeStruct(r.shape, r.dtype) for r in results),
         in_specs=[anyspace] * 4,
         out_specs=(anyspace,) * 4,
-        scratch_shapes=[dma((4,))],
+        scratch_shapes=[dma((4 + blocks * (batch // GROUP),))],
         compiler_params=pltpu.CompilerParams(vmem_limit_bytes=1024 * 1024),
     )(*results)
     return (*final[:3], final[3].swapaxes(1, 2))

time: 51.3 us -> 48.7 us (0.949)
  Pallas kernels: 50.5 us -> 47.9 us
    pallas_call x1, Pallas kernels: 42.9 us -> 40.5 us  [body(): pl.pallas_call(functools.partial(kernel, n), out_shape=(pltpu.VMEM((batch...]
where the time goes in v2:
time: 48.7 us; the launch traced here: 48.5 us
  Pallas kernels  47.9 us (98%)
  between operations  0.65 us (1%)
    pallas_call x1, Pallas kernels, body(): pl.pallas_call(functools.partial(kernel, n), out_shape=(pltpu.VMEM((batch...  40.5 us
    pallas_call x1, Pallas kernels, body(): pl.pallas_call(write_out, out_shape=tuple((jax.ShapeDtypeStruct(r.shape,...  7.33 us

profile of v2, /device:TPU:1, one launch (start us, length us, event | category | flops | bytes accessed | tf_op | source)
XLA Modules:
  0.0 48.5 jit_solution(9979557257766593997)
XLA Ops:
  0.6 40.5 %shard_map.192 = (bf16[80,128]{1,0:T(8,128)(2,1)S(1)}, f32[2,80,128,256]{3,2,1,0:T(8,128)S(1)}, f32[2,80,128]{2,1,0:T(8,128)S(1)}, f32[2,8,80]{2,1,0:T(8,128)S(1)}) custom-call(bf16[80,128]{1,0:T(8,128)(2,1)} %tokens.1, s32[1,80]{1,0:T(1,128)} %bitcast.8, f32[2,80,128,256]{3,2,1,0:T(8,128)} %cell_memory.1, f32[2,80,128]{2,1,0:T(8,128)} %key_sums.1, ...), custom_call_target="tpu_custom_call" | custom-call | tf_op jit(solution)/shard_map/pallas_call | solution.py:469
  41.2 7.3 %shard_map.193 = (bf16[80,128]{1,0:T(8,128)(2,1)}, f32[2,80,128,256]{3,2,1,0:T(8,128)}, f32[2,80,128]{2,1,0:T(8,128)}, f32[2,8,80]{2,1,0:T(8,128)}) custom-call(bf16[80,128]{1,0:T(8,128)(2,1)S(1)} %get-tuple-element.12.refs_0_, f32[2,80,128,256]{3,2,1,0:T(8,128)S(1)} %get-tuple-element.13.refs_1_, f32[2,80,128]{2,1,0:T(8,128)S(1)} %get-tuple-element.14.refs_2_, ...), custom_call_target="tpu_custom_call" | custom-call | tf_op jit(solution)/shard_map/pallas_call | solution.py:523
